TPU v7x, 32 devices: a whole 2x2x4 slice. The times are simulated.
32 devices in a mesh: sp: 16 (over z, y, x), tp: 2 (over core).
Axes of the slice: x: 2, y: 2, z: 4, core: 2. Of those that a mesh axis runs over, the one named last changes fastest.
Arguments:
- residual: bfloat16 [3072, 2048], P(('sp', 'tp')), may hold values from -6 to 6
- queries: bfloat16 [3072, 1024], P('sp', 'tp'), may hold values from -6 to 6
- key_pairs: bfloat16 [3072, 1024], P('sp', 'tp'), may hold values from -6 to 6
- values: bfloat16 [3072, 1024], P('sp', 'tp'), may hold values from -6 to 6
- second_weight: float32 [8], P('tp'), may hold values from 0.3 to 0.8
- head_gain: float32 [1024], P('tp'), may hold values from 0.1 to 1.9
- out_weight: bfloat16 [1024, 2048], P('tp'), may hold values from -0.1875 to 0.1875
- norm_gain: float32 [2048], replicated, may hold values from 0.1 to 1.9
- up_weight: bfloat16 [2048, 5632], P('sp', 'tp'), may hold values from -0.125 to 0.125
- gate_weight: bfloat16 [2048, 5632], P('sp', 'tp'), may hold values from -0.125 to 0.125
- conv_weight: float32 [3, 5632], P(None, 'tp'), may hold values from -3.5 to 3.5
- conv_bias: float32 [5632], P('tp'), may hold values from -3 to 3
- down_weight: bfloat16 [5632, 2048], P('tp', 'sp'), may hold values from -0.078125 to 0.078125
Outputs:
- layer_out: bfloat16 [3072, 2048], P(('sp', 'tp'))
All inputs are finite; a program needn't handle non-finite values.
Results may differ from a plain program's by a relative error of at most 0.017.
Values may be sent and summed in bfloat16 or wider, within the bound.
A program may use at most 128 MiB of HBM per device.

v0:
```python
import jax
import jax.numpy as jnp
from jax import lax
from jax.sharding import PartitionSpec as P

HD = 64
VD = 128
eps = 1e-05
neg_fill = -1e30


def from_behind(value, axis, steps):
    count = lax.axis_size(axis)
    leading, last = (max(0, -steps), min(count, count - steps))
    return lax.ppermute(value, axis, [(source, source + steps) for source in range(leading, last)])


def normalize(rows_in, gain):
    values_f = rows_in.astype(jnp.float32)
    scale_inv = lax.rsqrt(jnp.mean(values_f * values_f, axis=-1, keepdims=True) + eps)
    return (values_f * scale_inv * gain).astype(jnp.bfloat16)


def local(
    residual,
    queries,
    key_pairs,
    values,
    second_weight,
    head_gain,
    out_weight,
    norm_gain,
    up_weight,
    gate_weight,
    conv_weight,
    conv_bias,
    down_weight,
):
    tok_rows = queries.shape[0]
    head_count = second_weight.shape[0]
    ff_local = up_weight.shape[1]
    sp_index = lax.axis_index("sp")
    query = queries.reshape(tok_rows, head_count, 2, HD)
    query_pos = sp_index * tok_rows + jnp.arange(tok_rows)
    last_query = (sp_index + 1) * tok_rows
    initial = (
        jnp.full((head_count, 2, tok_rows), neg_fill, jnp.float32),
        jnp.zeros((head_count, 2, tok_rows), jnp.float32),
        jnp.zeros((head_count, 2, tok_rows, VD), jnp.float32),
    )
    key_piece = lax.all_gather(key_pairs, "sp", axis=0, tiled=True)
    value_piece = lax.all_gather(values, "sp", axis=0, tiled=True)
    piece_len = key_piece.shape[0]

    def compute(state_in):
        maxima, totals, weighted = state_in
        key_rows = key_piece.reshape(piece_len, head_count, 2, HD)
        value_rows = value_piece.reshape(piece_len, head_count, VD)
        scores = jnp.einsum(
            "qhmd,khmd->hmqk", query, key_rows, preferred_element_type=jnp.float32
        ) * HD ** (-0.5)
        visible = jnp.arange(piece_len)[None, :] <= query_pos[:, None]
        scores = jnp.where(visible, scores, neg_fill)
        new_max = jnp.maximum(maxima, jnp.max(scores, axis=-1))
        exp_scores = jnp.where(visible, jnp.exp(scores - new_max[..., None]), jnp.float32(0.0))
        totals = jnp.sum(exp_scores, axis=-1)
        weighted = jnp.einsum(
            "hmqk,khe->hmqe",
            exp_scores.astype(jnp.bfloat16),
            value_rows,
            preferred_element_type=jnp.float32,
        )
        return (new_max, totals, weighted)

    def keep_state(state_in):
        return state_in

    maxima, totals, weighted = lax.cond(jnp.int32(0) < last_query, compute, keep_state, initial)
    diff = (
        weighted[:, 0] / totals[:, 0, :, None]
        - second_weight[:, None, None] * weighted[:, 1] / totals[:, 1, :, None]
    )
    diff = jnp.transpose(diff, (1, 0, 2))
    scale_inv = lax.rsqrt(jnp.mean(diff * diff, axis=-1, keepdims=True) + eps)
    attended = (
        (diff * scale_inv * head_gain.reshape(head_count, VD) * 0.8)
        .reshape(tok_rows, head_count * VD)
        .astype(jnp.bfloat16)
    )
    proj = lax.psum_scatter(
        jnp.dot(attended, out_weight, preferred_element_type=jnp.float32).astype(jnp.bfloat16),
        "tp",
        scatter_dimension=0,
        tiled=True,
    )
    mid = (residual.astype(jnp.float32) + proj.astype(jnp.float32)).astype(jnp.bfloat16)
    normed_all = lax.all_gather(normalize(mid, norm_gain), "tp", axis=0, tiled=True)
    up_sum = jnp.dot(
        normed_all,
        lax.all_gather(up_weight, "sp", axis=0, tiled=True),
        preferred_element_type=jnp.float32,
    )
    gate_sum = jnp.dot(
        normed_all,
        lax.all_gather(gate_weight, "sp", axis=0, tiled=True),
        preferred_element_type=jnp.float32,
    )
    up_proj = up_sum.astype(jnp.bfloat16)
    gate_proj = gate_sum.astype(jnp.bfloat16)
    taps = conv_weight.shape[0]
    rim_rows = from_behind(up_proj[tok_rows - (taps - 1) :], "sp", 1)
    extended = jnp.concatenate((rim_rows, up_proj), axis=0)
    conv_out = jnp.zeros((tok_rows, ff_local), jnp.float32) + conv_bias[None, :]
    for tap in range(taps):
        conv_out = conv_out + conv_weight[tap][None, :] * extended[tap : tap + tok_rows].astype(
            jnp.float32
        )
    hidden = (jax.nn.silu(conv_out) * gate_proj.astype(jnp.float32)).astype(jnp.bfloat16)
    down_all = lax.all_gather(down_weight, "sp", axis=1, tiled=True)
    ffn_out = lax.psum_scatter(
        jnp.dot(hidden, down_all, preferred_element_type=jnp.float32).astype(jnp.bfloat16),
        "tp",
        scatter_dimension=0,
        tiled=True,
    )
    return (mid.astype(jnp.float32) + ffn_out.astype(jnp.float32)).astype(jnp.bfloat16)


def solution(mesh):
    return jax.shard_map(
        local,
        mesh=mesh,
        in_specs=(
            P(("sp", "tp"), None),
            P("sp", "tp"),
            P("sp", "tp"),
            P("sp", "tp"),
            P("tp"),
            P("tp"),
            P("tp", None),
            P(),
            P("sp", "tp"),
            P("sp", "tp"),
            P(None, "tp"),
            P("tp"),
            P("tp", "sp"),
        ),
        out_specs=P(("sp", "tp"), None),
        check_vma=False,
    )
```

profile of v0, /device:TPU:0, one launch (start us, length us, event | category | flops | bytes accessed | tf_op | source)
XLA Modules:
  0.0 705.0 jit_solution(9887044699763358971)
XLA Ops:
  6.5 0.7 all-gather.6.cloned.1.call-update
  7.3 0.7 all-gather.8.cloned.1.call-update
  8.1 72.7 %all-gather.6.cloned.1.call-done = bf16[3072,512]{1,0:T(8,128)(2,1)} async-done(((bf16[192,512]{1,0:T(8,128)(2,1)}), bf16[3072,512]{1,0:T(8,128)(2,1)}) %all-gather.6.cloned.1.call-update) | async-done | bytes 3145744 | tf_op jit(solution)/shard_map/all_gather | solution.py:51
  80.7 69.2 %all-gather.8.cloned.1.call-done = bf16[3072,512]{1,0:T(8,128)(2,1)} async-done(((bf16[192,512]{1,0:T(8,128)(2,1)}), bf16[3072,512]{1,0:T(8,128)(2,1)}) %all-gather.8.cloned.1.call-update) | async-done | bytes 3145744 | tf_op jit(solution)/shard_map/all_gather | solution.py:52
  150.0 45.3 %conditional.1 = (f32[4,2,192]{2,1,0:T(2,128)S(1)}, f32[4,2,192,128]{3,2,1,0:T(8,128)S(1)}) conditional(s32[]{:T(128)} %convert_element_type.62, () %tuple.13, (s32[]{:T(128)}, s32[192]{0:T(256)S(1)}, bf16[192,512]{1,0:T(8,128)(2,1)}, bf16[3072,512]{1,0:T(8,128)(2,1)}, bf16[3072,512]{1,0:T(8,128)(2,1)}) %tuple.14), branch_computations={%region_0.0_spmd, %region_1.4_spmd} | conditional | flops 1873869568 | bytes 80058688 | solution.py:78
  150.4 4.8 copy.26
  155.3 11.8 %fusion = (f32[4,2,192]{2,1,0:T(2,128)S(1)}, f32[4,2,192,3072]{3,2,1,0:T(8,128)}) fusion(pred[192,3072]{1,0:T(8,128)(4,1)S(1)} %iota_compare_fusion, bf16[192,4,2,64]{0,3,2,1:T(8,128)(2,1)S(1)} %bitcast.44, bf16[3072,4,2,64]{0,3,2,1:T(8,128)(2,1)} %bitcast.42), kind=kOutput, calls=%fused_computation.2 | convolution fusion | flops 618134016 | bytes 22812672 | tf_op jit(solution)/shard_map/cond/branch_1_fun/qhmd,khmd->hmqk/dot_general | solution.py:59
  167.1 5.5 reshape.37
  172.6 10.7 %fusion.3 = f32[4,2,192,128]{3,2,1,0:T(8,128)S(1)} fusion(f32[4,2,192,3072]{3,2,1,0:T(8,128)} %get-tuple-element.52, f32[4,2,192]{2,1,0:T(2,128)S(1)} %broadcast_maximum_fusion, pred[192,3072]{1,0:T(8,128)(4,1)S(1)} %iota_compare_fusion, bf16[3072,4,128,1]{2,1,0,3:T(4,128)(2,1)} %bitcast.43), kind=kOutput, calls=%fused_computation.5 | convolution fusion | flops 1231552512 | bytes 23402496 | tf_op jit(solution)/shard_map/cond/branch_1_fun/hmqk,khe->hmqe/dot_general | solution.py:67
  183.3 11.9 %fusion.2 = f32[4,2,192]{2,1,0:T(2,128)S(1)} fusion(f32[4,2,192,3072]{3,2,1,0:T(8,128)} %get-tuple-element.52, f32[4,2,192]{2,1,0:T(2,128)S(1)} %broadcast_maximum_fusion, pred[192,3072]{1,0:T(8,128)(4,1)S(1)} %iota_compare_fusion), kind=kLoop, calls=%fused_computation.4 | loop fusion | flops 23591424 | bytes 19476480 | tf_op jit(solution)/shard_map/cond/branch_1_fun/reduce_sum | solution.py:66
  195.8 1.5 convolution_convert_fusion.3
  198.0 0.5 all-gather.12.cloned.1.call-update
  199.1 5.1 reduce-scatter.3.cloned.1.call-done
  204.2 1.2 fusion.20
  205.5 1.2 fusion.22
  206.6 2.4 all_gather.20
  209.0 140.4 %all-gather.10.cloned.1.call-done = bf16[2048,2816]{1,0:T(8,128)(2,1)} async-done(((bf16[128,2816]{1,0:T(8,128)(2,1)}), bf16[2048,2816]{1,0:T(8,128)(2,1)}) %all-gather.10.cloned.1.call-update) | async-done | bytes 11534352 | tf_op jit(solution)/shard_map/all_gather | solution.py:100
  349.4 6.7 convolution_convert_fusion.1
  356.1 3.4 collective-permute-start
  359.6 132.0 %all-gather.12.cloned.1.call-done = bf16[2048,2816]{1,0:T(8,128)(2,1)} async-done(((bf16[128,2816]{1,0:T(8,128)(2,1)}), bf16[2048,2816]{1,0:T(8,128)(2,1)}) %all-gather.12.cloned.1.call-update) | async-done | bytes 11534352 | tf_op jit(solution)/shard_map/all_gather | solution.py:105
  491.6 182.8 %all-gather.14.cloned.1.call-done = bf16[2816,2048]{1,0:T(8,128)(2,1)} async-done(((bf16[2816,128]{1,0:T(8,128)(2,1)}), bf16[2816,2048]{1,0:T(8,128)(2,1)}) %all-gather.14.cloned.1.call-update) | async-done | bytes 11534352 | tf_op jit(solution)/shard_map/all_gather | solution.py:119
  674.5 15.2 %convolution_convert_fusion.2 = bf16[192,2048]{1,0:T(8,128)(2,1)} fusion(bf16[2816,2048]{1,0:T(8,128)(2,1)} %all-gather.14.cloned.1.call-done, bf16[192,2048]{1,0:T(8,128)(2,1)} %copy-done.4, bf16[2048,2816]{1,0:T(8,128)(2,1)} %all-gather.12.cloned.1.call-done, bf16[192,2816]{1,0:T(8,128)(2,1)} %copy-done.10, bf16[2,2816]{1,0:T(2,128)(2,1)S(1)} %collective-permute-done, ...), kind=kOutput, calls=%fused_computation.19 | convolution fusion | flops 4442013696 | bytes 25779200 | tf_op jit(solution)/shard_map/dot_general | solution.py:121
  689.7 6.5 reduce-scatter.5.cloned.1.call-done
  696.2 1.9 fusion.23
  (48 shorter events, 2.5 us)
Async XLA Ops:
  6.5 189.2 %copy-start = (bf16[512,2048]{1,0:T(8,128)(2,1)S(1)}, bf16[512,2048]{1,0:T(8,128)(2,1)}, u32[]{:S(2)}) copy-start(bf16[512,2048]{1,0:T(8,128)(2,1)} %param.21) | copy-start | bytes 6291460
  6.5 74.2 %all-gather.6.cloned.1.call-start = ((), (), s32[]{:S(2)}) async-start(), calls=%async_computation.2 | async-start | bytes 3342336 | tf_op jit(solution)/shard_map/all_gather | solution.py:51
  7.3 142.7 %all-gather.8.cloned.1.call-start = ((), (), s32[]{:S(2)}) async-start(), calls=%async_computation.3 | async-start | bytes 3342336 | tf_op jit(solution)/shard_map/all_gather | solution.py:52
  8.0 196.2 %reduce-scatter.3.cloned.1.call-start = ((), (), s32[]{:S(2)}) async-start(), calls=%async_computation.4 | async-start | bytes 1179648 | tf_op jit(solution)/shard_map/reduce_scatter | solution.py:90
  149.9 45.3 %copy-start.9 = (f32[4]{0:T(128)S(1)}, f32[4]{0:T(128)}, u32[]{:S(2)}) copy-start(f32[4]{0:T(128)} %param.19) | copy-start | bytes 52
  149.9 45.8 %copy-start.8 = (f32[512]{0:T(512)S(1)}, f32[512]{0:T(512)}, u32[]{:S(2)}) copy-start(f32[512]{0:T(512)} %param.20) | copy-start | bytes 6148
  150.3 4.8 copy-start.5
  195.7 8.5 %copy-start.2 = (bf16[96,2048]{1,0:T(8,128)(2,1)S(1)}, bf16[96,2048]{1,0:T(8,128)(2,1)}, u32[]{:S(2)}) copy-start(bf16[96,2048]{1,0:T(8,128)(2,1)} %param.15) | copy-start | bytes 1179652
  195.8 9.7 %copy-start.7 = (f32[2048]{0:T(1024)S(1)}, f32[2048]{0:T(1024)}, u32[]{:S(2)}) copy-start(f32[2048]{0:T(1024)} %param.22) | copy-start | bytes 24580
  197.4 152.0 %all-gather.10.cloned.1.call-start = ((), (), s32[]{:S(2)}) async-start(), calls=%async_computation.5 | async-start | bytes 12255232 | tf_op jit(solution)/shard_map/all_gather | solution.py:100
  197.9 293.7 %all-gather.12.cloned.1.call-start = ((), (), s32[]{:S(2)}) async-start(), calls=%async_computation.6 | async-start | bytes 12255232 | tf_op jit(solution)/shard_map/all_gather | solution.py:105
  198.5 475.9 %all-gather.14.cloned.1.call-start = ((), (), s32[]{:S(2)}) async-start(), calls=%async_computation.7 | async-start | bytes 12255232 | tf_op jit(solution)/shard_map/all_gather | solution.py:119
  199.1 497.1 %reduce-scatter.5.cloned.1.call-start = ((), (), s32[]{:S(2)}) async-start(), calls=%async_computation.8 | async-start | bytes 1179648 | tf_op jit(solution)/shard_map/reduce_scatter | solution.py:120
  209.0 147.1 %copy-start.4 = (bf16[192,2048]{1,0:T(8,128)(2,1)}, bf16[192,2048]{1,0:T(8,128)(2,1)S(1)}, u32[]{:S(2)}) copy-start(bf16[192,2048]{1,0:T(8,128)(2,1)S(1)} %all_gather.20) | copy-start | bytes 2359300
  209.0 150.5 %copy-start.6 = (f32[3,2816]{1,0:T(4,128)S(1)}, f32[3,2816]{1,0:T(4,128)}, u32[]{:S(2)}) copy-start(f32[3,2816]{1,0:T(4,128)} %param.25) | copy-start | bytes 101380
  209.0 465.5 %copy-start.11 = (f32[2816]{0:T(1024)S(1)}, f32[2816]{0:T(1024)}, u32[]{:S(2)}) copy-start(f32[2816]{0:T(1024)} %param.26) | copy-start | bytes 33796
  356.1 3.4 copy-start.10
  356.1 318.3 %collective-permute-start = (bf16[2,2816]{1,0:T(2,128)(2,1)S(1)}, bf16[2,2816]{1,0:T(2,128)(2,1)S(1)}, u32[]{:S(2)}, u32[]{:S(2)}) collective-permute-start(bf16[2,2816]{1,0:T(2,128)(2,1)S(1)} %slice.41), channel_id=1, source_target_pairs={{0,2},{2,4},{4,6},{6,8},{8,10},{10,12},{12,14},{14,16},{16,18},{18... | collective-permute-start | bytes 33800 | tf_op jit(solution)/shard_map/ppermute | solution.py:15
  674.5 21.8 %copy-start.3 = (bf16[96,2048]{1,0:T(8,128)(2,1)S(1)}, bf16[96,2048]{1,0:T(8,128)(2,1)}, u32[]{:S(2)}) copy-start(bf16[96,2048]{1,0:T(8,128)(2,1)} %reduce-scatter.3.cloned.1.call-done) | copy-start | bytes 1179652
  674.5 23.7 %copy-start.1 = (bf16[512,2048]{1,0:T(8,128)(2,1)S(1)}, bf16[512,2048]{1,0:T(8,128)(2,1)}, u32[]{:S(2)}) copy-start(bf16[512,2048]{1,0:T(8,128)(2,1)} %param.21) | copy-start | bytes 6291460
Sparse Core Ops, SparseCore 0:
  10.1 70.5 all-gather.5
  83.5 66.3 all-gather.7
  197.5 6.6 reduce-scatter.2
  206.8 142.5 all-gather.9
  352.0 139.5 all-gather.11
  494.2 180.2 all-gather.13
  689.8 6.3 reduce-scatter.4
where the time goes:
time: 706 us; the launch traced here: 705 us
  waiting for transfers between devices  612 us (87%)
  matrix products  45.9 us (7%)
  other arithmetic  17.1 us (2%)
  between operations  13.6 us (2%)
  local copies, waits for them, and re-layouts  10.6 us (2%)
    all_gather x1, waiting for transfers between devices, local(): down_all = lax.all_gather(down_weight, 'sp', axis=1, tiled=True)  183 us
    all_gather x1, waiting for transfers between devices, local(): lax.all_gather(up_weight, 'sp', axis=0, tiled=True)  140 us
    all_gather x1, waiting for transfers between devices, local(): lax.all_gather(gate_weight, 'sp', axis=0, tiled=True)  132 us
    all_gather x1, waiting for transfers between devices, local(): key_piece = lax.all_gather(key_pairs, 'sp', axis=0, tiled=True)  72.7 us
    all_gather x1, waiting for transfers between devices, local(): value_piece = lax.all_gather(values, 'sp', axis=0, tiled=True)  69.2 us
    dot_general x1, matrix products, local(): jnp.dot(hidden, down_all, preferred_element_type=jnp.float32)  15.2 us
  transfers between devices with their start and end apart: 8, of which 7 were waited for; matrix products, arithmetic and copies ran while one was open for 1% of the time, Pallas kernels for 0%

commit v1 on v0

--- a/solution.py
+++ b/solution.py
@@ -1,3 +1,4 @@
+import functools
 import jax
 import jax.numpy as jnp
 from jax import lax
@@ -7,6 +8,20 @@
 VD = 128
 eps = 1e-05
 neg_fill = -1e30
+
+
+def wall_serve(x_in, link_axis):
+    n_shards = jax.lax.psum(1, link_axis)
+    history = list(map(lambda i0: (i0, (i0 + 1) % n_shards), range(n_shards)))
+    block_next = [None] * n_shards
+    block_next[n_shards - 1] = x_in
+    for d in range(n_shards - 2, -1, -1):
+        block_next[d] = jax.lax.ppermute(block_next[d + 1], link_axis, history)
+    carry_out = jnp.concatenate(block_next, axis=1)
+    return jnp.roll(carry_out, (jax.lax.axis_index(link_axis) + 1) * x_in.shape[1], axis=1)
+
+
+read_outputs = functools.partial(wall_serve, link_axis="sp")
 
 
 def from_behind(value, axis, steps):
@@ -116,7 +131,7 @@
             jnp.float32
         )
     hidden = (jax.nn.silu(conv_out) * gate_proj.astype(jnp.float32)).astype(jnp.bfloat16)
-    down_all = lax.all_gather(down_weight, "sp", axis=1, tiled=True)
+    down_all = read_outputs(down_weight)
     ffn_out = lax.psum_scatter(
         jnp.dot(hidden, down_all, preferred_element_type=jnp.float32).astype(jnp.bfloat16),
         "tp",

time: 706 us -> 762 us (1.079)
  local copies, waits for them, and re-layouts: 10.6 us -> 68.6 us
    ppermute x0 -> x15, waiting for transfers between devices: none -> 457 us  [wall_serve(): block_next[d] = jax.lax.ppermute(block_next[d + 1], link_axis, history)]
    all_gather x1 -> x0, waiting for transfers between devices: 183 us -> none  [local(): down_all = lax.all_gather(down_weight, 'sp', axis=1, tiled=True)]
    all_gather x1, waiting for transfers between devices: 140 us -> 0.01 us  [local(): lax.all_gather(up_weight, 'sp', axis=0, tiled=True)]
    all_gather x1, waiting for transfers between devices: 132 us -> 0.01 us  [local(): lax.all_gather(gate_weight, 'sp', axis=0, tiled=True)]
    unnamed x23 -> x92, local copies, waits for them, and re-layouts: 0.05 us -> 56.3 us
  transfers between devices with their start and end apart: 8 -> 22, of which waited for: 7 -> 19; matrix products, arithmetic and copies ran while one was open for 1% -> 8% of each run, Pallas kernels for 0% -> 0%
where the time goes in v1:
time: 762 us; the launch traced here: 761 us
  waiting for transfers between devices  608 us (80%)
  local copies, waits for them, and re-layouts  68.6 us (9%)
  matrix products  46.7 us (6%)
  other arithmetic  18.4 us (2%)
  between operations  13.7 us (2%)
    ppermute x15, waiting for transfers between devices, wall_serve(): block_next[d] = jax.lax.ppermute(block_next[d + 1], link_axis, history)  457 us
    all_gather x1, waiting for transfers between devices, local(): key_piece = lax.all_gather(key_pairs, 'sp', axis=0, tiled=True)  72.7 us
    all_gather x1, waiting for transfers between devices, local(): value_piece = lax.all_gather(values, 'sp', axis=0, tiled=True)  69.2 us
    unnamed x92, local copies, waits for them, and re-layouts  56.3 us
  transfers between devices with their start and end apart: 22, of which 19 were waited for; matrix products, arithmetic and copies ran while one was open for 8% of the time, Pallas kernels for 0%

profile of v1, /device:TPU:0, one launch (start us, length us, event | category | flops | bytes accessed | tf_op | source)
XLA Modules:
  0.0 761.1 jit_solution(5334766728992978369)
XLA Ops:
  8.1 72.7 %all-gather.5.cloned.1.call-done = bf16[3072,512]{1,0:T(8,128)(2,1)} async-done(((bf16[192,512]{1,0:T(8,128)(2,1)}), bf16[3072,512]{1,0:T(8,128)(2,1)}) %all-gather.5.cloned.1.call-update) | async-done | bytes 3145744 | tf_op jit(solution)/shard_map/all_gather | solution.py:66
  80.7 69.2 %all-gather.7.cloned.1.call-done = bf16[3072,512]{1,0:T(8,128)(2,1)} async-done(((bf16[192,512]{1,0:T(8,128)(2,1)}), bf16[3072,512]{1,0:T(8,128)(2,1)}) %all-gather.7.cloned.1.call-update) | async-done | bytes 3145744 | tf_op jit(solution)/shard_map/all_gather | solution.py:67
  150.0 46.6 %conditional.1 = (f32[4,2,192]{2,1,0:T(2,128)S(1)}, f32[4,2,192,128]{3,2,1,0:T(8,128)}) conditional(s32[]{:T(128)} %convert_element_type.62, () %tuple.13, (s32[]{:T(128)}, s32[192]{0:T(256)S(1)}, bf16[192,512]{1,0:T(8,128)(2,1)}, bf16[3072,512]{1,0:T(8,128)(2,1)}, bf16[3072,512]{1,0:T(8,128)(2,1)}) %tuple.14), branch_computations={%region_0.0_spmd, %region_1.4_spmd} | conditional | flops 1873869568 | bytes 79272224 | solution.py:93
  156.1 11.8 %fusion = (f32[4,2,192]{2,1,0:T(2,128)S(1)}, f32[4,2,192,3072]{3,2,1,0:T(8,128)}) fusion(pred[192,3072]{1,0:T(8,128)(4,1)S(1)} %iota_compare_fusion, bf16[192,4,2,64]{0,3,2,1:T(8,128)(2,1)S(1)} %bitcast.43, bf16[3072,4,2,64]{0,3,2,1:T(8,128)(2,1)} %bitcast.41), kind=kOutput, calls=%fused_computation.2 | convolution fusion | flops 618134016 | bytes 22812672 | tf_op jit(solution)/shard_map/cond/branch_1_fun/qhmd,khmd->hmqk/dot_general | solution.py:74
  173.4 11.3 %fusion.3 = f32[4,2,192,128]{3,2,1,0:T(8,128)} fusion(f32[4,2,192,3072]{3,2,1,0:T(8,128)} %get-tuple-element.52, f32[4,2,192]{2,1,0:T(2,128)S(1)} %broadcast_maximum_fusion, pred[192,3072]{1,0:T(8,128)(4,1)S(1)} %iota_compare_fusion, bf16[3072,4,128,1]{2,1,0,3:T(4,128)(2,1)} %bitcast.42), kind=kOutput, calls=%fused_computation.5 | convolution fusion | flops 1231552512 | bytes 23402496 | tf_op jit(solution)/shard_map/cond/branch_1_fun/hmqk,khe->hmqe/dot_general | solution.py:82
  184.7 11.9 %fusion.2 = f32[4,2,192]{2,1,0:T(2,128)S(1)} fusion(f32[4,2,192,3072]{3,2,1,0:T(8,128)} %get-tuple-element.52, f32[4,2,192]{2,1,0:T(2,128)S(1)} %broadcast_maximum_fusion, pred[192,3072]{1,0:T(8,128)(4,1)S(1)} %iota_compare_fusion), kind=kLoop, calls=%fused_computation.4 | loop fusion | flops 23591424 | bytes 19476480 | tf_op jit(solution)/shard_map/cond/branch_1_fun/reduce_sum | solution.py:81
  202.1 18.3 %collective-permute-done.1 = bf16[2816,128]{1,0:T(8,128)(2,1)S(1)} collective-permute-done((bf16[2816,128]{1,0:T(8,128)(2,1)}, bf16[2816,128]{1,0:T(8,128)(2,1)S(1)}, u32[]{:S(2)}, u32[]{:S(2)}) %collective-permute-start.1) | collective-permute-done | bytes 720928 | tf_op jit(solution)/shard_map/ppermute | solution.py:19
  221.2 34.3 %collective-permute-done.2 = bf16[2816,128]{1,0:T(8,128)(2,1)} collective-permute-done((bf16[2816,128]{1,0:T(8,128)(2,1)S(1)}, bf16[2816,128]{1,0:T(8,128)(2,1)}, u32[]{:S(2)}, u32[]{:S(2)}) %collective-permute-start.2) | collective-permute-done | bytes 720928 | tf_op jit(solution)/shard_map/ppermute | solution.py:19
  255.6 35.9 %collective-permute-done.3 = bf16[2816,128]{1,0:T(8,128)(2,1)} collective-permute-done((bf16[2816,128]{1,0:T(8,128)(2,1)}, bf16[2816,128]{1,0:T(8,128)(2,1)}, u32[]{:S(2)}, u32[]{:S(2)}) %collective-permute-start.3) | collective-permute-done | bytes 720928 | tf_op jit(solution)/shard_map/ppermute | solution.py:19
  291.5 30.9 %collective-permute-done.4 = bf16[2816,128]{1,0:T(8,128)(2,1)S(1)} collective-permute-done((bf16[2816,128]{1,0:T(8,128)(2,1)}, bf16[2816,128]{1,0:T(8,128)(2,1)S(1)}, u32[]{:S(2)}, u32[]{:S(2)}) %collective-permute-start.4) | collective-permute-done | bytes 720928 | tf_op jit(solution)/shard_map/ppermute | solution.py:19
  323.3 37.0 %collective-permute-done.5 = bf16[2816,128]{1,0:T(8,128)(2,1)S(1)} collective-permute-done((bf16[2816,128]{1,0:T(8,128)(2,1)S(1)}, bf16[2816,128]{1,0:T(8,128)(2,1)S(1)}, u32[]{:S(2)}, u32[]{:S(2)}) %collective-permute-start.5) | collective-permute-done | bytes 720928 | tf_op jit(solution)/shard_map/ppermute | solution.py:19
  361.2 37.5 %collective-permute-done.6 = bf16[2816,128]{1,0:T(8,128)(2,1)S(1)} collective-permute-done((bf16[2816,128]{1,0:T(8,128)(2,1)S(1)}, bf16[2816,128]{1,0:T(8,128)(2,1)S(1)}, u32[]{:S(2)}, u32[]{:S(2)}) %collective-permute-start.6) | collective-permute-done | bytes 720928 | tf_op jit(solution)/shard_map/ppermute | solution.py:19
  399.6 34.5 %collective-permute-done.7 = bf16[2816,128]{1,0:T(8,128)(2,1)S(1)} collective-permute-done((bf16[2816,128]{1,0:T(8,128)(2,1)S(1)}, bf16[2816,128]{1,0:T(8,128)(2,1)S(1)}, u32[]{:S(2)}, u32[]{:S(2)}) %collective-permute-start.7) | collective-permute-done | bytes 720928 | tf_op jit(solution)/shard_map/ppermute | solution.py:19
  435.0 29.3 %collective-permute-done.8 = bf16[2816,128]{1,0:T(8,128)(2,1)S(1)} collective-permute-done((bf16[2816,128]{1,0:T(8,128)(2,1)S(1)}, bf16[2816,128]{1,0:T(8,128)(2,1)S(1)}, u32[]{:S(2)}, u32[]{:S(2)}) %collective-permute-start.8) | collective-permute-done | bytes 720928 | tf_op jit(solution)/shard_map/ppermute | solution.py:19
  465.1 26.7 %collective-permute-done.9 = bf16[2816,128]{1,0:T(8,128)(2,1)S(1)} collective-permute-done((bf16[2816,128]{1,0:T(8,128)(2,1)S(1)}, bf16[2816,128]{1,0:T(8,128)(2,1)S(1)}, u32[]{:S(2)}, u32[]{:S(2)}) %collective-permute-start.9) | collective-permute-done | bytes 720928 | tf_op jit(solution)/shard_map/ppermute | solution.py:19
  492.7 36.4 %collective-permute-done.10 = bf16[2816,128]{1,0:T(8,128)(2,1)S(1)} collective-permute-done((bf16[2816,128]{1,0:T(8,128)(2,1)S(1)}, bf16[2816,128]{1,0:T(8,128)(2,1)S(1)}, u32[]{:S(2)}, u32[]{:S(2)}) %collective-permute-start.10) | collective-permute-done | bytes 720928 | tf_op jit(solution)/shard_map/ppermute | solution.py:19
  530.0 25.9 %collective-permute-done.11 = bf16[2816,128]{1,0:T(8,128)(2,1)S(1)} collective-permute-done((bf16[2816,128]{1,0:T(8,128)(2,1)S(1)}, bf16[2816,128]{1,0:T(8,128)(2,1)S(1)}, u32[]{:S(2)}, u32[]{:S(2)}) %collective-permute-start.11) | collective-permute-done | bytes 720928 | tf_op jit(solution)/shard_map/ppermute | solution.py:19
  556.7 35.9 %collective-permute-done.12 = bf16[2816,128]{1,0:T(8,128)(2,1)S(1)} collective-permute-done((bf16[2816,128]{1,0:T(8,128)(2,1)S(1)}, bf16[2816,128]{1,0:T(8,128)(2,1)S(1)}, u32[]{:S(2)}, u32[]{:S(2)}) %collective-permute-start.12) | collective-permute-done | bytes 720928 | tf_op jit(solution)/shard_map/ppermute | solution.py:19
  593.4 35.9 %collective-permute-done.13 = bf16[2816,128]{1,0:T(8,128)(2,1)} collective-permute-done((bf16[2816,128]{1,0:T(8,128)(2,1)S(1)}, bf16[2816,128]{1,0:T(8,128)(2,1)}, u32[]{:S(2)}, u32[]{:S(2)}) %collective-permute-start.13) | collective-permute-done | bytes 720928 | tf_op jit(solution)/shard_map/ppermute | solution.py:19
  631.0 26.9 %collective-permute-done.14 = bf16[2816,128]{1,0:T(8,128)(2,1)} collective-permute-done((bf16[2816,128]{1,0:T(8,128)(2,1)}, bf16[2816,128]{1,0:T(8,128)(2,1)}, u32[]{:S(2)}, u32[]{:S(2)}) %collective-permute-start.14) | collective-permute-done | bytes 720928 | tf_op jit(solution)/shard_map/ppermute | solution.py:19
  662.0 11.1 %collective-permute-done.15 = bf16[2816,128]{1,0:T(8,128)(2,1)S(1)} collective-permute-done((bf16[2816,128]{1,0:T(8,128)(2,1)}, bf16[2816,128]{1,0:T(8,128)(2,1)S(1)}, u32[]{:S(2)}, u32[]{:S(2)}) %collective-permute-start.15) | collective-permute-done | bytes 720928 | tf_op jit(solution)/shard_map/ppermute | solution.py:19
  720.7 6.9 convolution_convert_fusion.1
  730.4 15.1 %fusion.15 = bf16[192,2048]{1,0:T(8,128)(2,1)} fusion(bf16[2816,4096]{1,0:T(8,128)(2,1)} %constant_dynamic-update-slice_fusion, s32[]{:T(128)S(6)} %select_n.22, bf16[192,2048]{1,0:T(8,128)(2,1)} %all_gather.17, bf16[2048,2816]{1,0:T(8,128)(2,1)} %all-gather.11.cloned.1.call-done, bf16[192,2816]{1,0:T(8,128)(2,1)} %copy-done.28, ...), kind=kOutput, calls=%fused_computation.21 | convolution fusion | flops 4442013696 | bytes 25779204 | tf_op jit(solution)/shard_map/dot_general | solution.py:136
  745.5 6.9 reduce-scatter.5.cloned.1.call-done
  (143 shorter events, 84.9 us)
Async XLA Ops:
  6.5 74.2 %all-gather.5.cloned.1.call-start = ((), (), s32[]{:S(2)}) async-start(), calls=%async_computation.2 | async-start | bytes 3342336 | tf_op jit(solution)/shard_map/all_gather | solution.py:66
  7.3 142.7 %all-gather.7.cloned.1.call-start = ((), (), s32[]{:S(2)}) async-start(), calls=%async_computation.3 | async-start | bytes 3342336 | tf_op jit(solution)/shard_map/all_gather | solution.py:67
  8.0 621.5 %reduce-scatter.3.cloned.1.call-start = ((), (), s32[]{:S(2)}) async-start(), calls=%async_computation.4 | async-start | bytes 1179648 | tf_op jit(solution)/shard_map/reduce_scatter | solution.py:105
  150.0 508.0 %copy-start.25 = (f32[2048]{0:T(1024)S(1)}, f32[2048]{0:T(1024)}, u32[]{:S(2)}) copy-start(f32[2048]{0:T(1024)} %param.22) | copy-start | bytes 24580
  196.6 504.2 %copy-start.3 = (bf16[2816,128]{1,0:T(8,128)(2,1)S(1)}, bf16[2816,128]{1,0:T(8,128)(2,1)}, u32[]{:S(2)}) copy-start(bf16[2816,128]{1,0:T(8,128)(2,1)} %param.27) | copy-start | bytes 2162692
  199.9 520.8 %all-gather.9.cloned.1.call-start = ((), (), s32[]{:S(2)}) async-start(), calls=%async_computation.5 | async-start | bytes 12255232 | tf_op jit(solution)/shard_map/all_gather | solution.py:115
  200.5 529.5 %all-gather.11.cloned.1.call-start = ((), (), s32[]{:S(2)}) async-start(), calls=%async_computation.6 | async-start | bytes 12255232 | tf_op jit(solution)/shard_map/all_gather | solution.py:120
  200.5 19.8 %collective-permute-start.1 = (bf16[2816,128]{1,0:T(8,128)(2,1)}, bf16[2816,128]{1,0:T(8,128)(2,1)S(1)}, u32[]{:S(2)}, u32[]{:S(2)}) collective-permute-start(bf16[2816,128]{1,0:T(8,128)(2,1)} %param.27), channel_id=1, source_target_pairs={{0,2},{2,4},{4,6},{6,8},{8,10},{10,12},{12,14},{14,16},{16,18},{18... | collective-permute-start | bytes 2162696 | tf_op jit(solution)/shard_map/ppermute | solution.py:19
  221.2 34.3 %collective-permute-start.2 = (bf16[2816,128]{1,0:T(8,128)(2,1)S(1)}, bf16[2816,128]{1,0:T(8,128)(2,1)}, u32[]{:S(2)}, u32[]{:S(2)}) collective-permute-start(bf16[2816,128]{1,0:T(8,128)(2,1)S(1)} %collective-permute-done.1), channel_id=1, source_target_pairs={{0,2},{2,4},{4,6},{6,8},{8,10},{10,12},{12,14},{14,16},{16,18},{18... | collective-permute-start | bytes 2162696 | tf_op jit(solution)/shard_map/ppermute | solution.py:19
  255.5 36.0 %collective-permute-start.3 = (bf16[2816,128]{1,0:T(8,128)(2,1)}, bf16[2816,128]{1,0:T(8,128)(2,1)}, u32[]{:S(2)}, u32[]{:S(2)}) collective-permute-start(bf16[2816,128]{1,0:T(8,128)(2,1)} %collective-permute-done.2), channel_id=1, source_target_pairs={{0,2},{2,4},{4,6},{6,8},{8,10},{10,12},{12,14},{14,16},{16,18},{18... | collective-permute-start | bytes 2162696 | tf_op jit(solution)/shard_map/ppermute | solution.py:19
  255.5 496.9 %reduce-scatter.5.cloned.1.call-start = ((), (), s32[]{:S(2)}) async-start(), calls=%async_computation.7 | async-start | bytes 1179648 | tf_op jit(solution)/shard_map/reduce_scatter | solution.py:135
  291.5 30.9 %collective-permute-start.4 = (bf16[2816,128]{1,0:T(8,128)(2,1)}, bf16[2816,128]{1,0:T(8,128)(2,1)S(1)}, u32[]{:S(2)}, u32[]{:S(2)}) collective-permute-start(bf16[2816,128]{1,0:T(8,128)(2,1)} %collective-permute-done.3), channel_id=1, source_target_pairs={{0,2},{2,4},{4,6},{6,8},{8,10},{10,12},{12,14},{14,16},{16,18},{18... | collective-permute-start | bytes 2162696 | tf_op jit(solution)/shard_map/ppermute | solution.py:19
  323.3 37.0 %collective-permute-start.5 = (bf16[2816,128]{1,0:T(8,128)(2,1)S(1)}, bf16[2816,128]{1,0:T(8,128)(2,1)S(1)}, u32[]{:S(2)}, u32[]{:S(2)}) collective-permute-start(bf16[2816,128]{1,0:T(8,128)(2,1)S(1)} %collective-permute-done.4), channel_id=1, source_target_pairs={{0,2},{2,4},{4,6},{6,8},{8,10},{10,12},{12,14},{14,16},{16,18},{18... | collective-permute-start | bytes 2162696 | tf_op jit(solution)/shard_map/ppermute | solution.py:19
  361.2 37.5 %collective-permute-start.6 = (bf16[2816,128]{1,0:T(8,128)(2,1)S(1)}, bf16[2816,128]{1,0:T(8,128)(2,1)S(1)}, u32[]{:S(2)}, u32[]{:S(2)}) collective-permute-start(bf16[2816,128]{1,0:T(8,128)(2,1)S(1)} %collective-permute-done.5), channel_id=1, source_target_pairs={{0,2},{2,4},{4,6},{6,8},{8,10},{10,12},{12,14},{14,16},{16,18},{18... | collective-permute-start | bytes 2162696 | tf_op jit(solution)/shard_map/ppermute | solution.py:19
  399.6 34.5 %collective-permute-start.7 = (bf16[2816,128]{1,0:T(8,128)(2,1)S(1)}, bf16[2816,128]{1,0:T(8,128)(2,1)S(1)}, u32[]{:S(2)}, u32[]{:S(2)}) collective-permute-start(bf16[2816,128]{1,0:T(8,128)(2,1)S(1)} %collective-permute-done.6), channel_id=1, source_target_pairs={{0,2},{2,4},{4,6},{6,8},{8,10},{10,12},{12,14},{14,16},{16,18},{18... | collective-permute-start | bytes 2162696 | tf_op jit(solution)/shard_map/ppermute | solution.py:19
  435.0 29.3 %collective-permute-start.8 = (bf16[2816,128]{1,0:T(8,128)(2,1)S(1)}, bf16[2816,128]{1,0:T(8,128)(2,1)S(1)}, u32[]{:S(2)}, u32[]{:S(2)}) collective-permute-start(bf16[2816,128]{1,0:T(8,128)(2,1)S(1)} %collective-permute-done.7), channel_id=1, source_target_pairs={{0,2},{2,4},{4,6},{6,8},{8,10},{10,12},{12,14},{14,16},{16,18},{18... | collective-permute-start | bytes 2162696 | tf_op jit(solution)/shard_map/ppermute | solution.py:19
  465.1 26.7 %collective-permute-start.9 = (bf16[2816,128]{1,0:T(8,128)(2,1)S(1)}, bf16[2816,128]{1,0:T(8,128)(2,1)S(1)}, u32[]{:S(2)}, u32[]{:S(2)}) collective-permute-start(bf16[2816,128]{1,0:T(8,128)(2,1)S(1)} %collective-permute-done.8), channel_id=1, source_target_pairs={{0,2},{2,4},{4,6},{6,8},{8,10},{10,12},{12,14},{14,16},{16,18},{18... | collective-permute-start | bytes 2162696 | tf_op jit(solution)/shard_map/ppermute | solution.py:19
  492.6 36.4 %collective-permute-start.10 = (bf16[2816,128]{1,0:T(8,128)(2,1)S(1)}, bf16[2816,128]{1,0:T(8,128)(2,1)S(1)}, u32[]{:S(2)}, u32[]{:S(2)}) collective-permute-start(bf16[2816,128]{1,0:T(8,128)(2,1)S(1)} %collective-permute-done.9), channel_id=1, source_target_pairs={{0,2},{2,4},{4,6},{6,8},{8,10},{10,12},{12,14},{14,16},{16,18},{18... | collective-permute-start | bytes 2162696 | tf_op jit(solution)/shard_map/ppermute | solution.py:19
  530.0 25.9 %collective-permute-start.11 = (bf16[2816,128]{1,0:T(8,128)(2,1)S(1)}, bf16[2816,128]{1,0:T(8,128)(2,1)S(1)}, u32[]{:S(2)}, u32[]{:S(2)}) collective-permute-start(bf16[2816,128]{1,0:T(8,128)(2,1)S(1)} %collective-permute-done.10), channel_id=1, source_target_pairs={{0,2},{2,4},{4,6},{6,8},{8,10},{10,12},{12,14},{14,16},{16,18},{18... | collective-permute-start | bytes 2162696 | tf_op jit(solution)/shard_map/ppermute | solution.py:19
  556.7 35.9 %collective-permute-start.12 = (bf16[2816,128]{1,0:T(8,128)(2,1)S(1)}, bf16[2816,128]{1,0:T(8,128)(2,1)S(1)}, u32[]{:S(2)}, u32[]{:S(2)}) collective-permute-start(bf16[2816,128]{1,0:T(8,128)(2,1)S(1)} %collective-permute-done.11), channel_id=1, source_target_pairs={{0,2},{2,4},{4,6},{6,8},{8,10},{10,12},{12,14},{14,16},{16,18},{18... | collective-permute-start | bytes 2162696 | tf_op jit(solution)/shard_map/ppermute | solution.py:19
  593.4 36.0 %collective-permute-start.13 = (bf16[2816,128]{1,0:T(8,128)(2,1)S(1)}, bf16[2816,128]{1,0:T(8,128)(2,1)}, u32[]{:S(2)}, u32[]{:S(2)}) collective-permute-start(bf16[2816,128]{1,0:T(8,128)(2,1)S(1)} %collective-permute-done.12), channel_id=1, source_target_pairs={{0,2},{2,4},{4,6},{6,8},{8,10},{10,12},{12,14},{14,16},{16,18},{18... | collective-permute-start | bytes 2162696 | tf_op jit(solution)/shard_map/ppermute | solution.py:19
  629.4 28.5 %collective-permute-start.14 = (bf16[2816,128]{1,0:T(8,128)(2,1)}, bf16[2816,128]{1,0:T(8,128)(2,1)}, u32[]{:S(2)}, u32[]{:S(2)}) collective-permute-start(bf16[2816,128]{1,0:T(8,128)(2,1)} %collective-permute-done.13), channel_id=1, source_target_pairs={{0,2},{2,4},{4,6},{6,8},{8,10},{10,12},{12,14},{14,16},{16,18},{18... | collective-permute-start | bytes 2162696 | tf_op jit(solution)/shard_map/ppermute | solution.py:19
  657.9 15.1 %collective-permute-start.15 = (bf16[2816,128]{1,0:T(8,128)(2,1)}, bf16[2816,128]{1,0:T(8,128)(2,1)S(1)}, u32[]{:S(2)}, u32[]{:S(2)}) collective-permute-start(bf16[2816,128]{1,0:T(8,128)(2,1)} %collective-permute-done.14), channel_id=1, source_target_pairs={{0,2},{2,4},{4,6},{6,8},{8,10},{10,12},{12,14},{14,16},{16,18},{18... | collective-permute-start | bytes 2162696 | tf_op jit(solution)/shard_map/ppermute | solution.py:19
  727.7 2.7 collective-permute-start
  (28 other events, 2020.0 us)
Sparse Core Ops, SparseCore 0:
  10.1 70.5 all-gather.4
  83.5 66.3 all-gather.6
  200.0 6.6 reduce-scatter.2
  209.4 208.3 all-gather.8
  420.4 219.7 all-gather.10
  745.7 6.6 reduce-scatter.4
